TPU v7x, 512 devices: a whole 4x4x16 slice. The times are simulated.
512 devices in a mesh: ep: 128 (over z, x, core), tp: 4 (over y).
Axes of the slice: x: 4, y: 4, z: 16, core: 2. Of those that a mesh axis runs over, the one named last changes fastest.
Arguments:
- tokens: bfloat16 [16384, 2048], P('ep'), may hold values from -6 to 6
- norm_gain: float32 [2048], replicated, may hold values from 0.1 to 1.9
- expert_ids: int32 [16384, 2], P('ep'), may hold values from 0 to 31, all different within a row; in each aligned block of 128 rows (0 to 127, 128 to 255, ...) at most 12 rows name the same one
- gate_weights: float32 [16384, 2], P('ep'), may hold values from 0.2 to 1
- w_gate: bfloat16 [2048, 131072], P(None, ('ep', 'tp')), may hold values from -0.125 to 0.125
- w_up: bfloat16 [2048, 131072], P(None, ('ep', 'tp')), may hold values from -0.125 to 0.125
- w_down: bfloat16 [131072, 2048], P('ep', 'tp'), may hold values from -0.09375 to 0.09375
Outputs:
- moe_out: bfloat16 [16384, 2048], P('ep', 'tp')
Inputs may be any that keep to these rules, and one draw needn't show every extreme that they name: `expert_ids`: each token names 2 different experts; in each aligned block of 128 rows no expert is named by more than 12 rows, a bound that some block reaches.
All inputs are finite; a program needn't handle non-finite values.
Results may differ from a plain program's by a relative error of at most 0.0071.
Values may be sent and summed in bfloat16 or wider, within the bound.
No kernel may reach another device: no remote copies, remote signals or barrier semaphores. Data moves between devices by JAX's collectives and lax.ppermute only.
A program may use at most 64 MiB of HBM per device.

v0:
```python
import jax
import jax.numpy as jnp
from jax import lax
from jax.sharding import Mesh
from jax.sharding import PartitionSpec as P

TOP = 2
EP = ("ep_0", "ep_1", "ep_2")
EP_TP = ("ep_0", "ep_1", "ep_2", "tp")
EPS = 1e-06


def split_up(array, dim, length):
    lengths = array.shape
    parts = array.reshape(*lengths[:dim], length, lengths[dim] // length, *lengths[dim + 1 :])
    return jnp.moveaxis(parts, dim, 0)


def laid_out(parts, dim):
    parts = jnp.moveaxis(parts, 0, dim)
    lengths = parts.shape
    return parts.reshape(*lengths[:dim], lengths[dim] * lengths[dim + 1], *lengths[dim + 2 :])


def turned_blocks(parts, axes, sequence):
    inside = parts.shape[1:]
    out = parts.reshape(*(lax.axis_size(a) for a in axes), *inside)
    for k in sequence:
        out = lax.all_to_all(out, axes[k], k, k, tiled=True)
    return out.reshape(-1, *inside)


def exchange_by_chip(array, groups, sequence, split_dim, concat_dim):
    length = lax.axis_size(groups[0]) * lax.axis_size(groups[1])
    parts = split_up(array, split_dim, length)
    return laid_out(turned_blocks(parts, groups, sequence), concat_dim)


def rms_rows(values, gain):
    widened = values.astype(jnp.float32)
    scale = lax.rsqrt(jnp.mean(widened * widened, axis=-1, keepdims=True) + EPS)
    return (widened * scale * gain).astype(jnp.bfloat16)


def on_device(tokens, norm_gain, expert_ids, gate_weights, w_gate, w_up, w_down):
    ep_count = lax.axis_size(EP)
    tp_count = lax.axis_size("tp")
    row_count = tokens.shape[0]
    group_size = max(1, ep_count // 32)
    expert_count = ep_count // group_size
    share = (row_count * TOP * 5 + 4 * expert_count * tp_count - 1) // (4 * expert_count * tp_count)
    capacity = min(row_count, tp_count * share)
    normed = rms_rows(tokens, norm_gain)
    flat_ids = expert_ids.reshape(-1)
    matches = (flat_ids[:, None] == jnp.arange(expert_count, dtype=jnp.int32)[None, :]).astype(
        jnp.int32
    )
    slot_index = jnp.sum((jnp.cumsum(matches, axis=0) - matches) * matches, axis=1)
    position = flat_ids * capacity + slot_index
    placing = (
        position[:, None] == jnp.arange(expert_count * capacity, dtype=jnp.int32)[None, :]
    ).astype(jnp.float32)
    placing = placing.reshape(row_count, TOP, expert_count * capacity)
    selector = jnp.sum(placing, axis=1).astype(jnp.bfloat16)
    buffers = lax.dot_general(
        selector, normed, (((0,), (0,)), ((), ())), preferred_element_type=jnp.float32
    )
    buffers = buffers.astype(jnp.bfloat16).reshape(expert_count, capacity, -1)
    quarter = capacity // tp_count
    mine = lax.dynamic_slice_in_dim(buffers, lax.axis_index("tp") * quarter, quarter, 1)
    copies = jnp.repeat(mine, group_size, axis=0)
    arrived = exchange_by_chip(copies, (("ep_0", "ep_1"), "ep_2"), (1, 0), 0, 0)
    received = lax.all_gather(arrived, "tp", axis=1, tiled=True)
    sources, slot_count, model_width = received.shape
    flat_rows = received.reshape(sources * slot_count, model_width)
    gate_proj = jnp.dot(flat_rows, w_gate, preferred_element_type=jnp.float32)
    upper = jnp.dot(flat_rows, w_up, preferred_element_type=jnp.float32)
    hidden = (jax.nn.silu(gate_proj) * upper).astype(jnp.bfloat16)
    partial_out = jnp.dot(
        lax.all_gather(hidden, "tp", axis=1, tiled=True), w_down, preferred_element_type=jnp.float32
    ).astype(jnp.bfloat16)
    partial_out = partial_out.reshape(sources, slot_count, w_down.shape[1])
    sources, slot_count, out_width = partial_out.shape
    back = exchange_by_chip(partial_out, (("ep_0", "ep_1"), "ep_2"), (1, 0), 0, 0)
    back = back.reshape(expert_count, group_size, slot_count, out_width).astype(jnp.float32)
    returned = jnp.sum(back, axis=1)
    summed = returned.reshape(expert_count * capacity, -1)
    combine = jnp.sum(placing * gate_weights[:, :, None], axis=1)
    mixed = jnp.dot(
        combine, summed, precision=lax.Precision.HIGHEST, preferred_element_type=jnp.float32
    )
    return mixed.astype(jnp.bfloat16)


def solution(mesh):
    finer = Mesh(mesh.devices.reshape(16, 4, 2, mesh.shape["tp"]), ("ep_0", "ep_1", "ep_2", "tp"))
    placed = (
        P(EP, None),
        P(),
        P(EP, None),
        P(EP, None),
        P(None, EP_TP),
        P(None, EP_TP),
        P(EP, "tp"),
    )
    return jax.shard_map(
        on_device, mesh=finer, in_specs=placed, out_specs=P(EP, "tp"), check_vma=False
    )
```

profile of v0, /device:TPU:2, one launch (start us, length us, event | category | flops | bytes accessed | tf_op | source)
XLA Modules:
  0.0 389.9 jit_solution(7729169001689056819)
XLA Ops:
  6.5 0.0 copy-start
  6.5 0.0 all-gather.3.cloned.1.call-start
  6.5 0.9 copy.81
  7.4 0.1 eq.43
  7.6 0.1 eq.39
  7.7 1.2 fusion.1
  9.0 0.6 reduce-window.6
  9.6 0.2 slice_reduce_fusion
  9.8 0.1 fusion.10
  9.9 0.1 reduce_sum.55
  10.1 0.1 copy.84
  10.1 0.7 multiply_add_fusion
  10.8 0.8 convert_reduce_fusion.1
  11.7 0.0 copy-done.2
  11.7 1.4 convolution_convert_fusion.1
  13.1 1.5 reshape.57
  14.6 2.0 constant_dynamic-slice_fusion
  16.6 0.3 copy.85
  16.9 0.5 broadcast_in_dim.6
  17.4 0.3 broadcast_in_dim.14
  17.7 0.2 broadcast_in_dim.15
  17.8 5.0 %all_to_all.20 = bf16[64,2,1,3,2048]{4,0,3,2,1:T(8,128)(2,1)S(1)} all-to-all(bf16[64,2,1,3,2048]{4,0,3,2,1:T(8,128)(2,1)S(1)} %broadcast_in_dim.15), channel_id=1, replica_groups=mesh['ep_0'=16,'ep_1'=4,'ep_2'=2,'tp'=4] {'ep_2'}, dimensions={1} | all-to-all | bytes 3145728 | tf_op jit(solution)/shard_map/all_to_all | solution.py:29
  22.8 1.6 copy.86
  24.5 96.4 %all_to_all.21 = bf16[64,2,1,3,2048]{4,1,3,2,0:T(2,128)(2,1)S(1)} all-to-all(bf16[64,2,1,3,2048]{4,1,3,2,0:T(2,128)(2,1)S(1)} %copy.86), channel_id=1, replica_groups=mesh['ep_0'=16,'ep_1'=4,'ep_2'=2,'tp'=4] {'ep_0','ep_1'}, dimensions={0} | all-to-all | bytes 3145728 | tf_op jit(solution)/shard_map/all_to_all | solution.py:29
  120.8 1.1 copy.87
  122.0 2.0 reshape_reshape.3
  124.0 0.0 all-gather.3.cloned.1.call-update
  124.0 0.2 all-gather.5.cloned.1.call-start
  124.3 65.0 %all-gather.3.cloned.1.call-done = bf16[128,12,2048]{2,0,1:T(8,128)(2,1)} async-done(((bf16[128,3,2048]{2,0,1:T(8,128)(2,1)}), bf16[128,12,2048]{2,0,1:T(8,128)(2,1)}) %all-gather.3.cloned.1.call-update) | async-done | bytes 6291472 | tf_op jit(solution)/shard_map/all_gather | solution.py:73
  189.3 9.7 %copy.88 = bf16[128,12,2048]{2,1,0:T(8,128)(2,1)} copy(bf16[128,12,2048]{2,0,1:T(8,128)(2,1)} %all-gather.3.cloned.1.call-done) | data formatting | bytes 12582912 | tf_op jit(solution)/shard_map/all_gather | solution.py:73
  198.9 10.8 %reshape.58 = bf16[1536,2048]{1,0:T(8,128)(2,1)} reshape(bf16[128,12,2048]{2,1,0:T(8,128)(2,1)} %copy.88) | data formatting | bytes 12582912 | tf_op jit(solution)/shard_map/reshape | solution.py:75
  209.7 0.0 copy-done.3
  209.7 4.8 %fusion.12 = f32[1536,256]{1,0:T(8,128)S(1)} fusion(bf16[1536,2048]{1,0:T(8,128)(2,1)} %reshape.58, bf16[2048,256]{1,0:T(8,128)(2,1)S(1)} %copy-done.3), kind=kOutput, calls=%fused_computation.30 | convolution fusion | flops 1610612736 | bytes 8912896 | tf_op jit(solution)/shard_map/dot_general | solution.py:76
  214.6 0.0 copy-done.1
  214.6 0.0 copy-done.4
  214.6 3.0 fusion
  217.5 0.0 all-gather.5.cloned.1.call-update
  217.6 51.2 %all-gather.5.cloned.1.call-done = bf16[1536,1024]{1,0:T(8,128)(2,1)} async-done(((bf16[1536,256]{1,0:T(8,128)(2,1)}), bf16[1536,1024]{1,0:T(8,128)(2,1)}) %all-gather.5.cloned.1.call-update) | async-done | bytes 3145744 | tf_op jit(solution)/shard_map/all_gather | solution.py:80
  268.8 4.8 %convolution_convert_fusion = bf16[1536,512]{1,0:T(8,128)(2,1)} fusion(bf16[1536,1024]{1,0:T(8,128)(2,1)} %all-gather.5.cloned.1.call-done, bf16[1024,512]{1,0:T(8,128)(2,1)S(1)} %copy-done), kind=kOutput, calls=%fused_computation.1 | convolution fusion | flops 1611399168 | bytes 5767168 | tf_op jit(solution)/shard_map/dot_general | solution.py:79
  273.6 2.4 reshape_reshape_reshape.2
  276.0 0.9 copy.89
  276.8 5.0 %all_to_all.22 = bf16[64,2,1,12,512]{4,0,3,2,1:T(8,128)(2,1)S(1)} all-to-all(bf16[64,2,1,12,512]{4,0,3,2,1:T(8,128)(2,1)S(1)} %copy.89), channel_id=1, replica_groups=mesh['ep_0'=16,'ep_1'=4,'ep_2'=2,'tp'=4] {'ep_2'}, dimensions={1} | all-to-all | bytes 3145728 | tf_op jit(solution)/shard_map/all_to_all | solution.py:29
  281.8 1.6 copy.90
  283.5 93.7 %all_to_all.23 = bf16[64,2,1,12,512]{4,1,3,2,0:T(2,128)(2,1)S(1)} all-to-all(bf16[64,2,1,12,512]{4,1,3,2,0:T(2,128)(2,1)S(1)} %copy.90), channel_id=1, replica_groups=mesh['ep_0'=16,'ep_1'=4,'ep_2'=2,'tp'=4] {'ep_0','ep_1'}, dimensions={0} | all-to-all | bytes 3145728 | tf_op jit(solution)/shard_map/all_to_all | solution.py:29
  377.1 4.2 %convert_reduce_fusion = f32[64,12,512]{2,1,0:T(8,128)S(1)} fusion(bf16[64,2,1,12,512]{4,1,3,2,0:T(2,128)(2,1)S(1)} %all_to_all.23), kind=kLoop, calls=%fused_computation | loop fusion | flops 1179648 | bytes 3145728 | tf_op jit(solution)/shard_map/reduce_sum | solution.py:86
  381.4 0.3 bitcast_reduce_fusion
  381.6 0.1 reshape.59
  381.7 1.3 convolution_convert_fusion.2
  (9 shorter events, 0.1 us)
Async XLA Ops:
  6.5 262.3 %copy-start = (bf16[1024,512]{1,0:T(8,128)(2,1)S(1)}, bf16[1024,512]{1,0:T(8,128)(2,1)}, u32[]{:S(2)}) copy-start(bf16[1024,512]{1,0:T(8,128)(2,1)} %param.13) | copy-start | bytes 3145732
  6.5 5.1 %copy-start.2 = (bf16[128,2048]{1,0:T(8,128)(2,1)S(1)}, bf16[128,2048]{1,0:T(8,128)(2,1)}, u32[]{:S(2)}) copy-start(bf16[128,2048]{1,0:T(8,128)(2,1)} %param.7) | copy-start | bytes 1572868
  6.5 182.7 %all-gather.3.cloned.1.call-start = ((), (), s32[]{:S(2)}) async-start(), calls=%async_computation.4 | async-start | bytes 7864320 | tf_op jit(solution)/shard_map/all_gather | solution.py:73
  124.0 144.7 %all-gather.5.cloned.1.call-start = ((), (), s32[]{:S(2)}) async-start(), calls=%async_computation.5 | async-start | bytes 3932160 | tf_op jit(solution)/shard_map/all_gather | solution.py:80
  198.9 10.8 %copy-start.3 = (bf16[2048,256]{1,0:T(8,128)(2,1)S(1)}, bf16[2048,256]{1,0:T(8,128)(2,1)}, u32[]{:S(2)}) copy-start(bf16[2048,256]{1,0:T(8,128)(2,1)} %param.11) | copy-start | bytes 3145732
  209.7 4.8 %copy-start.1 = (bf16[1536,2048]{1,0:T(8,128)(2,1)S(1)}, bf16[1536,2048]{1,0:T(8,128)(2,1)}, u32[]{:S(2)}) copy-start(bf16[1536,2048]{1,0:T(8,128)(2,1)} %reshape.58) | copy-start | bytes 18874372
  209.7 4.9 %copy-start.4 = (bf16[2048,256]{1,0:T(8,128)(2,1)S(1)}, bf16[2048,256]{1,0:T(8,128)(2,1)}, u32[]{:S(2)}) copy-start(bf16[2048,256]{1,0:T(8,128)(2,1)} %param.12) | copy-start | bytes 3145732
Sparse Core Ops, SparseCore 0:
  124.2 65.0 all-gather.2
  217.7 51.0 all-gather.4
where the time goes:
time: 391 us; the launch traced here: 390 us
  blocking collectives  200 us (51%)
  waiting for transfers between devices  116 us (30%)
  local copies, waits for them, and re-layouts  36.5 us (9%)
  matrix products  15.2 us (4%)
  between operations  13.6 us (3%)
  other arithmetic  8.01 us (2%)
    all_to_all x4, blocking collectives, turned_blocks(): out = lax.all_to_all(out, axes[k], k, k, tiled=True)  200 us
    all_gather x1, waiting for transfers between devices, on_device(): received = lax.all_gather(arrived, 'tp', axis=1, tiled=True)  65 us
    all_gather x1, waiting for transfers between devices, on_device(): lax.all_gather(hidden, 'tp', axis=1, tiled=True)  51.2 us
    reshape x1, local copies, waits for them, and re-layouts, on_device(): flat_rows = received.reshape(sources * slot_count, model_width)  10.8 us
    all_gather x1, local copies, waits for them, and re-layouts, on_device(): received = lax.all_gather(arrived, 'tp', axis=1, tiled=True)  9.65 us
  transfers between devices with their start and end apart: 2, of which 2 were waited for; matrix products, arithmetic and copies ran while one was open for 0% of the time, Pallas kernels for 0%

commit v1 on v0

--- a/solution.py
+++ b/solution.py
@@ -77,7 +77,11 @@
     upper = jnp.dot(flat_rows, w_up, preferred_element_type=jnp.float32)
     hidden = (jax.nn.silu(gate_proj) * upper).astype(jnp.bfloat16)
     partial_out = jnp.dot(
-        lax.all_gather(hidden, "tp", axis=1, tiled=True), w_down, preferred_element_type=jnp.float32
+        jnp.concatenate(
+            lax.all_to_all(jnp.stack([hidden] * lax.axis_size("tp")), "tp", 0, 0), axis=1
+        ),
+        w_down,
+        preferred_element_type=jnp.float32,
     ).astype(jnp.bfloat16)
     partial_out = partial_out.reshape(sources, slot_count, w_down.shape[1])
     sources, slot_count, out_width = partial_out.shape

time: 391 us -> 378 us (0.967)
  waiting for transfers between devices: 116 us -> 65.3 us
  blocking collectives: 200 us -> 241 us
    all_gather x1 -> x0, waiting for transfers between devices: 51.2 us -> none  [on_device(): lax.all_gather(hidden, 'tp', axis=1, tiled=True)]
    all_to_all x0 -> x1, blocking collectives: none -> 40.9 us  [on_device(): lax.all_to_all(jnp.stack([hidden] * lax.axis_size('tp')), 'tp', 0, 0)]
  transfers between devices with their start and end apart: 2 -> 1, of which waited for: 2 -> 1; matrix products, arithmetic and copies ran while one was open for 0% -> 0% of each run, Pallas kernels for 0% -> 0%
where the time goes in v1:
time: 378 us; the launch traced here: 377 us
  blocking collectives  241 us (64%)
  waiting for transfers between devices  65.3 us (17%)
  local copies, waits for them, and re-layouts  37 us (10%)
  between operations  13.6 us (4%)
  matrix products  12.5 us (3%)
  other arithmetic  8.01 us (2%)
    all_to_all x4, blocking collectives, turned_blocks(): out = lax.all_to_all(out, axes[k], k, k, tiled=True)  200 us
    all_gather x1, waiting for transfers between devices, on_device(): received = lax.all_gather(arrived, 'tp', axis=1, tiled=True)  65.3 us
    all_to_all x1, blocking collectives, on_device(): lax.all_to_all(jnp.stack([hidden] * lax.axis_size('tp')), 'tp', 0, 0)  40.9 us
    reshape x1, local copies, waits for them, and re-layouts, on_device(): flat_rows = received.reshape(sources * slot_count, model_width)  10.8 us
    all_gather x1, local copies, waits for them, and re-layouts, on_device(): received = lax.all_gather(arrived, 'tp', axis=1, tiled=True)  9.65 us
  transfers between devices with their start and end apart: 1, of which 1 were waited for; matrix products, arithmetic and copies ran while one was open for 0% of the time, Pallas kernels for 0%

profile of v1, /device:TPU:2, one launch (start us, length us, event | category | flops | bytes accessed | tf_op | source)
XLA Modules:
  0.0 377.1 jit_solution(13730696275977817900)
XLA Ops:
  6.5 0.0 copy-start
  6.5 0.0 all-gather.2.cloned.1.call-start
  6.5 0.9 copy.87
  7.4 0.1 eq.43
  7.6 0.1 eq.39
  7.7 1.2 fusion.1
  9.0 0.6 reduce-window.6
  9.6 0.2 slice_reduce_fusion
  9.8 0.1 fusion.10
  9.9 0.1 reduce_sum.55
  10.1 0.1 copy.90
  10.1 0.7 multiply_add_fusion
  10.8 0.8 convert_reduce_fusion.1
  11.7 0.0 copy-done.2
  11.7 1.4 convolution_convert_fusion.1
  13.1 1.5 reshape.65
  14.6 2.0 constant_dynamic-slice_fusion
  16.6 0.3 copy.91
  16.9 0.5 broadcast_in_dim.6
  17.4 0.3 broadcast_in_dim.14
  17.7 0.2 broadcast_in_dim.15
  17.8 5.0 %all_to_all.25 = bf16[64,2,1,3,2048]{4,0,3,2,1:T(8,128)(2,1)S(1)} all-to-all(bf16[64,2,1,3,2048]{4,0,3,2,1:T(8,128)(2,1)S(1)} %broadcast_in_dim.15), channel_id=1, replica_groups=mesh['ep_0'=16,'ep_1'=4,'ep_2'=2,'tp'=4] {'ep_2'}, dimensions={1} | all-to-all | bytes 3145728 | tf_op jit(solution)/shard_map/all_to_all | solution.py:29
  22.8 1.6 copy.92
  24.5 96.4 %all_to_all.26 = bf16[64,2,1,3,2048]{4,1,3,2,0:T(2,128)(2,1)S(1)} all-to-all(bf16[64,2,1,3,2048]{4,1,3,2,0:T(2,128)(2,1)S(1)} %copy.92), channel_id=1, replica_groups=mesh['ep_0'=16,'ep_1'=4,'ep_2'=2,'tp'=4] {'ep_0','ep_1'}, dimensions={0} | all-to-all | bytes 3145728 | tf_op jit(solution)/shard_map/all_to_all | solution.py:29
  120.8 1.1 copy.93
  122.0 2.0 reshape_reshape.3
  124.0 0.0 all-gather.2.cloned.1.call-update
  124.0 65.3 %all-gather.2.cloned.1.call-done = bf16[128,12,2048]{2,0,1:T(8,128)(2,1)} async-done(((bf16[128,3,2048]{2,0,1:T(8,128)(2,1)}), bf16[128,12,2048]{2,0,1:T(8,128)(2,1)}) %all-gather.2.cloned.1.call-update) | async-done | bytes 6291472 | tf_op jit(solution)/shard_map/all_gather | solution.py:73
  189.3 9.7 %copy.94 = bf16[128,12,2048]{2,1,0:T(8,128)(2,1)} copy(bf16[128,12,2048]{2,0,1:T(8,128)(2,1)} %all-gather.2.cloned.1.call-done) | data formatting | bytes 12582912 | tf_op jit(solution)/shard_map/all_gather | solution.py:73
  198.9 10.8 %reshape.66 = bf16[1536,2048]{1,0:T(8,128)(2,1)} reshape(bf16[128,12,2048]{2,1,0:T(8,128)(2,1)} %copy.94) | data formatting | bytes 12582912 | tf_op jit(solution)/shard_map/reshape | solution.py:75
  209.7 0.0 copy-done.3
  209.7 4.8 %fusion.12 = f32[1536,256]{1,0:T(8,128)S(1)} fusion(bf16[1536,2048]{1,0:T(8,128)(2,1)} %reshape.66, bf16[2048,256]{1,0:T(8,128)(2,1)S(1)} %copy-done.3), kind=kOutput, calls=%fused_computation.30 | convolution fusion | flops 1610612736 | bytes 8912896 | tf_op jit(solution)/shard_map/dot_general | solution.py:76
  214.6 0.0 copy-done.4
  214.6 2.1 fusion
  216.7 0.3 copy.95
  217.0 0.2 stack.2
  217.2 40.9 %all_to_all.27 = bf16[4,1536,256]{1,2,0:T(8,128)(2,1)S(1)} all-to-all(bf16[4,1536,256]{1,2,0:T(8,128)(2,1)S(1)} %stack.2), channel_id=1, replica_groups=mesh['ep_0'=16,'ep_1'=4,'ep_2'=2,'tp'=4] {'tp'}, dimensions={0} | all-to-all | bytes 6291456 | tf_op jit(solution)/shard_map/all_to_all | solution.py:81
  258.1 0.0 copy-done
  258.1 3.0 convolution_convert_fusion
  261.0 2.4 reshape_reshape_reshape.2
  263.4 0.9 copy.96
  264.3 5.0 %all_to_all.28 = bf16[64,2,1,12,512]{4,0,3,2,1:T(8,128)(2,1)S(1)} all-to-all(bf16[64,2,1,12,512]{4,0,3,2,1:T(8,128)(2,1)S(1)} %copy.96), channel_id=1, replica_groups=mesh['ep_0'=16,'ep_1'=4,'ep_2'=2,'tp'=4] {'ep_2'}, dimensions={1} | all-to-all | bytes 3145728 | tf_op jit(solution)/shard_map/all_to_all | solution.py:29
  269.3 1.6 copy.97
  270.9 93.5 %all_to_all.29 = bf16[64,2,1,12,512]{4,1,3,2,0:T(2,128)(2,1)S(1)} all-to-all(bf16[64,2,1,12,512]{4,1,3,2,0:T(2,128)(2,1)S(1)} %copy.97), channel_id=1, replica_groups=mesh['ep_0'=16,'ep_1'=4,'ep_2'=2,'tp'=4] {'ep_0','ep_1'}, dimensions={0} | all-to-all | bytes 3145728 | tf_op jit(solution)/shard_map/all_to_all | solution.py:29
  364.4 4.2 %convert_reduce_fusion = f32[64,12,512]{2,1,0:T(8,128)S(1)} fusion(bf16[64,2,1,12,512]{4,1,3,2,0:T(2,128)(2,1)S(1)} %all_to_all.29), kind=kLoop, calls=%fused_computation | loop fusion | flops 1179648 | bytes 3145728 | tf_op jit(solution)/shard_map/reduce_sum | solution.py:90
  368.6 0.3 bitcast_reduce_fusion
  368.8 0.1 reshape.69
  368.9 1.3 convolution_convert_fusion.2
  (9 shorter events, 0.1 us)
Async XLA Ops:
  6.5 251.5 %copy-start = (bf16[1024,512]{1,0:T(8,128)(2,1)S(1)}, bf16[1024,512]{1,0:T(8,128)(2,1)}, u32[]{:S(2)}) copy-start(bf16[1024,512]{1,0:T(8,128)(2,1)} %param.13) | copy-start | bytes 3145732
  6.5 5.1 %copy-start.2 = (bf16[128,2048]{1,0:T(8,128)(2,1)S(1)}, bf16[128,2048]{1,0:T(8,128)(2,1)}, u32[]{:S(2)}) copy-start(bf16[128,2048]{1,0:T(8,128)(2,1)} %param.7) | copy-start | bytes 1572868
  6.5 182.7 %all-gather.2.cloned.1.call-start = ((), (), s32[]{:S(2)}) async-start(), calls=%async_computation.5 | async-start | bytes 7864320 | tf_op jit(solution)/shard_map/all_gather | solution.py:73
  198.9 10.8 %copy-start.3 = (bf16[2048,256]{1,0:T(8,128)(2,1)S(1)}, bf16[2048,256]{1,0:T(8,128)(2,1)}, u32[]{:S(2)}) copy-start(bf16[2048,256]{1,0:T(8,128)(2,1)} %param.11) | copy-start | bytes 3145732
  209.7 4.8 %copy-start.1 = (bf16[1536,2048]{1,0:T(8,128)(2,1)S(1)}, bf16[1536,2048]{1,0:T(8,128)(2,1)}, u32[]{:S(2)}) copy-start(bf16[1536,2048]{1,0:T(8,128)(2,1)} %reshape.66) | copy-start | bytes 18874372
  209.7 4.9 %copy-start.4 = (bf16[2048,256]{1,0:T(8,128)(2,1)S(1)}, bf16[2048,256]{1,0:T(8,128)(2,1)}, u32[]{:S(2)}) copy-start(bf16[2048,256]{1,0:T(8,128)(2,1)} %param.12) | copy-start | bytes 3145732
Sparse Core Ops, SparseCore 0:
  124.2 65.0 all-gather.1
